TPU v7x, 256 devices: a whole 4x4x8 slice. The times are simulated.
256 devices in a mesh: ep: 64 (over z, y, core), tp: 4 (over x).
Axes of the slice: x: 4, y: 4, z: 8, core: 2. Of those that a mesh axis runs over, the one named last changes fastest.
Arguments:
- tokens: bfloat16 [2048, 2048], P('ep'), may hold values from -6 to 6
- gain_mix: bfloat16 [2048], replicated, may hold values from 0.099609375 to 1.8984375
- gain_ffn: bfloat16 [2048], replicated, may hold values from 0.099609375 to 1.8984375
- w_query: bfloat16 [2048, 1024], P('ep', 'tp'), may hold values from -0.125 to 0.125
- w_key: bfloat16 [2048, 1024], P('ep', 'tp'), may hold values from -0.125 to 0.125
- w_value: bfloat16 [2048, 1024], P('ep', 'tp'), may hold values from -0.125 to 0.125
- w_outgate: bfloat16 [2048, 1024], P('ep', 'tp'), may hold values from -0.125 to 0.125
- w_ingate: bfloat16 [2048, 8], replicated, may hold values from -0.125 to 0.125
- w_forget: bfloat16 [2048, 8], replicated, may hold values from -0.125 to 0.125
- bias_in: float32 [8], replicated, may hold values from -2 to 2
- bias_forget: float32 [8], replicated, may hold values from -1 to 3
- w_proj: bfloat16 [1024, 2048], P('tp'), may hold values from -0.1875 to 0.1875
- matrix_state: float32 [2048, 8, 128, 128], P('ep', 'tp'), may hold values from -0.6 to 0.6
- normal_state: float32 [2048, 8, 128], P('ep', 'tp'), may hold values from -0.6 to 0.6
- stab_state: float32 [2048, 8], P('ep', 'tp'), may hold values from -1 to 1
- route_ids: int32 [2048, 2], P('ep'), may hold values from 0 to 31, all different within a row; in each aligned block of 32 rows (0 to 31, 32 to 63, ...) at most 4 rows name the same one
- route_weights: float32 [2048, 2], P('ep'), may hold values from 0.1 to 1
- w_exp_gate: bfloat16 [64, 2048, 1536], P('ep', None, 'tp'), may hold values from -0.125 to 0.125
- w_exp_up: bfloat16 [64, 2048, 1536], P('ep', None, 'tp'), may hold values from -0.125 to 0.125
- w_exp_down: bfloat16 [64, 1536, 2048], P('ep', 'tp'), may hold values from -0.109375 to 0.109375
Outputs:
- mixed_out: bfloat16 [2048, 2048], P('ep', 'tp')
- matrix_out: float32 [2048, 8, 128, 128], P('ep', 'tp')
- normal_out: float32 [2048, 8, 128], P('ep', 'tp')
- stab_out: float32 [2048, 8], P('ep', 'tp')
Inputs may be any that keep to these rules, and one draw needn't show every extreme that they name: `route_ids`: each row names 2 different experts; among the rows of one index of ep no expert is named by more than 4 rows, and in every draw some expert is named by exactly 4 of them.
All inputs are finite; a program needn't handle non-finite values.
Results may differ from a plain program's by a relative error of at most 0.015.
Values may be sent and summed in bfloat16 or wider, within the bound.
A program may use at most 64 MiB of HBM per device.

v0:
```python
import jax
import jax.numpy as jnp
from jax import lax
from jax.sharding import PartitionSpec as P

norm_epsilon = 1e-06


def in_one_piece(arrays, axis, dim, along):
    ends, at = ([], 0)
    for a in arrays[:-1]:
        at += a.shape[along]
        ends.append(at)
    both = jnp.concatenate(arrays, axis=along)
    return tuple(jnp.split(lax.all_gather(both, axis, axis=dim, tiled=True), ends, axis=along))


def copy_for_each(shard, axis):
    copies = jnp.broadcast_to(shard, (lax.axis_size(axis), *shard.shape))
    return lax.all_to_all(copies, axis, split_axis=0, concat_axis=0, tiled=True)


def of_everyone(shard, axis):
    everything = copy_for_each(shard, axis)
    return jnp.sum(everything.astype(jnp.float32), axis=0)


def split_up(shard, dim, length):
    shape = shard.shape
    tiles = shard.reshape(*shape[:dim], length, shape[dim] // length, *shape[dim + 1 :])
    return jnp.moveaxis(tiles, dim, 0)


def sum_at_owner(shard, axis, dim):
    length = lax.axis_size(axis)
    tiles = lax.all_to_all(split_up(shard, dim, length), axis, 0, 0, tiled=True)
    return jnp.sum(tiles.astype(jnp.float32), axis=0)


def rms_scale(row_block, gain):
    wide = row_block.astype(jnp.float32)
    factor = lax.rsqrt(jnp.mean(wide * wide, axis=-1, keepdims=True) + norm_epsilon)
    return (wide * factor * gain.astype(jnp.float32)).astype(jnp.bfloat16)


def memory_step(
    query,
    key_rows,
    value_rows,
    gate_rows,
    in_pre,
    forget_pre,
    matrix_state,
    normal_state,
    stab_state,
):
    log_forget = jax.nn.log_sigmoid(forget_pre)
    stab_new = jnp.maximum(log_forget + stab_state, in_pre)
    carry = jnp.exp(log_forget + stab_state - stab_new)
    inflow = jnp.exp(in_pre - stab_new)
    scaled_keys = key_rows.astype(jnp.float32) * query.shape[-1] ** (-0.5)
    value_wide = value_rows.astype(jnp.float32)
    matrix_new = (
        carry[..., None, None] * matrix_state
        + inflow[..., None, None] * scaled_keys[..., :, None] * value_wide[..., None, :]
    )
    normal_new = carry[..., None] * normal_state + inflow[..., None] * scaled_keys
    query_wide = query.astype(jnp.float32)
    numer = jnp.einsum("shd,shde->she", query_wide, matrix_new)
    denom = jnp.maximum(jnp.abs(jnp.sum(query_wide * normal_new, axis=-1)), 1.0)
    hidden = numer / denom[..., None] * jax.nn.sigmoid(gate_rows.astype(jnp.float32))
    return (hidden, matrix_new, normal_new, stab_new)


def dispatch_table(route_ids, experts, capacity):
    flat_ids = route_ids.reshape(-1)
    expert_hot = (flat_ids[:, None] == jnp.arange(experts, dtype=jnp.int32)[None, :]).astype(
        jnp.int32
    )
    slot_rank = jnp.sum((jnp.cumsum(expert_hot, axis=0) - 1) * expert_hot, axis=1)
    slot_hot = (slot_rank[:, None] == jnp.arange(capacity, dtype=jnp.int32)[None, :]).astype(
        jnp.float32
    )
    table = expert_hot.astype(jnp.float32)[:, :, None] * slot_hot[:, None, :]
    return table.reshape(flat_ids.shape[0], experts * capacity)


def send_rows(table, row_block, top_count, experts, capacity):
    repeated = jnp.repeat(row_block, top_count, axis=0)
    packed = jnp.einsum(
        "as,aw->sw", table.astype(jnp.bfloat16), repeated, preferred_element_type=jnp.float32
    ).astype(jnp.bfloat16)
    row_width = row_block.shape[1]
    doubled = jnp.broadcast_to(
        packed.reshape(experts, 1, capacity, row_width), (experts, 2, capacity, row_width)
    )
    return doubled.reshape(experts * 2 * capacity, row_width)


def body(
    tokens,
    gain_mix,
    gain_ffn,
    w_query,
    w_key,
    w_value,
    w_outgate,
    w_ingate,
    w_forget,
    bias_in,
    bias_forget,
    w_proj,
    matrix_state,
    normal_state,
    stab_state,
    route_ids,
    route_weights,
    w_exp_gate,
    w_exp_up,
    w_exp_down,
):
    ep_count = lax.axis_size("ep")
    tp_count = lax.axis_size("tp")
    tp_index = lax.axis_index("tp")
    seq_dev = tokens.shape[0]
    model_width = tokens.shape[1]
    heads_dev = matrix_state.shape[1]
    head_dim = matrix_state.shape[2]
    head_cols = w_query.shape[1]
    top_count = route_ids.shape[1]
    experts = ep_count // 2
    capacity = min(seq_dev, max(2, 2 * seq_dev * top_count // experts))
    col_width = model_width // tp_count
    normed = rms_scale(tokens, gain_mix)
    weight_pieces = in_one_piece((w_query, w_key, w_value, w_outgate), "ep", 0, 1)
    partials = tuple(
        (
            jnp.dot(normed, weight_piece, preferred_element_type=jnp.float32)
            for weight_piece in weight_pieces
        )
    )
    query, key_rows, value_rows, gate_rows = [
        partial_value.astype(jnp.bfloat16).reshape(seq_dev, heads_dev, head_dim)
        for partial_value in partials
    ]
    head_first = tp_index * heads_dev
    in_pre = lax.dynamic_slice_in_dim(
        jnp.dot(normed, w_ingate, preferred_element_type=jnp.float32) + bias_in,
        head_first,
        heads_dev,
        1,
    )
    forget_pre = lax.dynamic_slice_in_dim(
        jnp.dot(normed, w_forget, preferred_element_type=jnp.float32) + bias_forget,
        head_first,
        heads_dev,
        1,
    )
    hidden, matrix_new, normal_new, stab_new = memory_step(
        query,
        key_rows,
        value_rows,
        gate_rows,
        in_pre,
        forget_pre,
        matrix_state,
        normal_state,
        stab_state,
    )
    cell = hidden.reshape(seq_dev, head_cols).astype(jnp.bfloat16)
    partial_out = jnp.dot(cell, w_proj, preferred_element_type=jnp.float32)
    table = dispatch_table(route_ids, experts, capacity)
    gate_local = w_exp_gate[0]
    up_local = w_exp_up[0]
    attended = of_everyone(partial_out.astype(jnp.bfloat16), "tp").astype(jnp.float32)
    resid = (tokens.astype(jnp.float32) + attended).astype(jnp.bfloat16)
    normed_ffn = rms_scale(resid, gain_ffn)
    own_resid = lax.dynamic_slice_in_dim(resid, tp_index * col_width, col_width, 1)
    outgoing = send_rows(table, normed_ffn, top_count, experts, capacity)
    received = lax.all_to_all(outgoing, "ep", split_axis=0, concat_axis=0, tiled=True)
    gate_sum = jnp.dot(received, gate_local, preferred_element_type=jnp.float32)
    up_sum = jnp.dot(received, up_local, preferred_element_type=jnp.float32)
    inner = (jax.nn.silu(gate_sum) * up_sum).astype(jnp.bfloat16)
    expert_terms = jnp.dot(inner, w_exp_down[0], preferred_element_type=jnp.float32)
    half_share = sum_at_owner(expert_terms.astype(jnp.bfloat16), "tp", 1).astype(jnp.bfloat16)
    returned = lax.all_to_all(half_share, "ep", split_axis=0, concat_axis=0, tiled=True)
    halves_summed = jnp.sum(
        returned.astype(jnp.float32).reshape(experts, 2, capacity, col_width), axis=1
    ).reshape(experts * capacity, col_width)
    weights = route_weights / jnp.sum(route_weights, axis=-1, keepdims=True)
    combine = jnp.sum(
        (table * weights.reshape(-1)[:, None]).reshape(seq_dev, top_count, experts * capacity),
        axis=1,
    )
    routed = jnp.dot(combine, halves_summed)
    mixed_out = (own_resid.astype(jnp.float32) + routed).astype(jnp.bfloat16)
    return (mixed_out, matrix_new, normal_new, stab_new)


def solution(mesh):
    placed = (
        P("ep", None),
        P(),
        P(),
        P("ep", "tp"),
        P("ep", "tp"),
        P("ep", "tp"),
        P("ep", "tp"),
        P(),
        P(),
        P(),
        P(),
        P("tp", None),
        P("ep", "tp", None, None),
        P("ep", "tp", None),
        P("ep", "tp"),
        P("ep", None),
        P("ep", None),
        P("ep", None, "tp"),
        P("ep", None, "tp"),
        P("ep", "tp", None),
    )
    return jax.shard_map(
        body,
        mesh=mesh,
        in_specs=placed,
        out_specs=(P("ep", "tp"), P("ep", "tp", None, None), P("ep", "tp", None), P("ep", "tp")),
        check_vma=False,
    )
```

profile of v0, /device:TPU:1, one launch (start us, length us, event | category | flops | bytes accessed | tf_op | source)
XLA Modules:
  0.0 214.2 jit_solution(6402215370408316755)
XLA Ops:
  7.2 1.5 pad_maximum_fusion
  8.8 0.7 convert_element_type.131
  9.5 0.7 convert_element_type.155
  10.2 1.0 fusion.33
  11.2 1.2 convolution_add_fusion.1
  12.4 1.1 convolution_add_fusion.2
  13.5 0.7 subtract_exponential_fusion
  14.4 0.8 copy.55
  15.7 79.1 %all-gather.2.cloned.1.call-done = bf16[2048,1024]{1,0:T(8,128)(2,1)} async-done(((bf16[32,1024]{1,0:T(8,128)(2,1)}), bf16[2048,1024]{1,0:T(8,128)(2,1)}) %all-gather.2.cloned.1.call-update) | async-done | bytes 4194320 | tf_op jit(solution)/shard_map/all_gather | solution.py:15
  94.8 1.6 convolution_convert_fusion.6
  96.5 1.6 fusion.18
  98.1 1.5 fusion.20
  99.7 1.5 fusion.19
  101.3 0.8 multiply_reduce_fusion.1
  102.1 3.7 %multiply_add_fusion = f32[32,2,128,128]{3,2,1,0:T(8,128)S(1)} fusion(f32[32,2,128,128]{3,2,1,0:T(8,128)} %param.32, f32[32,2,128]{2,1,0:T(2,128)S(1)} %reshape.161, f32[32,2,128]{2,1,0:T(2,128)S(1)} %get-tuple-element.8, f32[32,2]{1,0:T(8,128)S(1)} %copy.52), kind=kLoop, calls=%fused_computation | loop fusion | flops 3145728 | bytes 8454400 | tf_op jit(solution)/shard_map/add | solution.py:64
  105.8 2.0 copy-done.1
  107.8 0.7 fusion.57
  109.3 0.8 broadcast_in_dim.8
  110.2 4.0 %all-to-all-start = ((bf16[4,32,2048]{2,1,0:T(8,128)(2,1)}), bf16[4,32,2048]{2,1,0:T(8,128)(2,1)S(1)}, u32[]{:S(2)}, u32[]{:S(2)}) async-start(bf16[4,32,2048]{2,1,0:T(8,128)(2,1)} %broadcast_in_dim.8), calls=%async_computation | async-start | bytes 1048576 | tf_op jit(solution)/shard_map/all_to_all | solution.py:20
  114.2 9.0 %all-to-all-done = bf16[4,32,2048]{2,1,0:T(8,128)(2,1)S(1)} async-done(((bf16[4,32,2048]{2,1,0:T(8,128)(2,1)}), bf16[4,32,2048]{2,1,0:T(8,128)(2,1)S(1)}, u32[]{:S(2)}, u32[]{:S(2)}) %all-to-all-start) | async-done | bytes 524320 | tf_op jit(solution)/shard_map/all_to_all | solution.py:20
  124.8 35.2 %all_to_all.31 = bf16[64,4,2048]{2,1,0:T(4,128)(2,1)} all-to-all(bf16[64,4,2048]{2,1,0:T(4,128)(2,1)S(1)} %bitcast.44), channel_id=1, replica_groups=mesh['ep'=64,'tp'=4] {'ep'}, dimensions={0} | all-to-all | bytes 2097152 | tf_op jit(solution)/shard_map/all_to_all | solution.py:180
  159.9 1.3 all_to_all.23
  161.3 2.1 fusion.3
  163.4 3.7 %convolution_convert_fusion = bf16[256,2048]{1,0:T(8,128)(2,1)} fusion(bf16[1,384,2048]{2,1,0:T(8,128)(2,1)S(1)} %copy-done, bf16[256,2048]{1,0:T(8,128)(2,1)S(1)} %all_to_all.23, bf16[1,2048,384]{2,1,0:T(8,128)(2,1)} %param.38, f32[256,384]{1,0:T(8,128)S(1)} %fusion.3), kind=kOutput, calls=%fused_computation.1 | convolution fusion | flops 806420480 | bytes 5636096 | tf_op jit(solution)/shard_map/dot_general | solution.py:184
  167.1 1.3 copy.72
  168.5 16.5 %all_to_all.32 = bf16[4,256,512]{2,1,0:T(8,128)(2,1)S(1)} all-to-all(bf16[4,256,512]{2,1,0:T(8,128)(2,1)S(1)} %bitcast.45), channel_id=1, replica_groups=mesh['ep'=64,'tp'=4] {'tp'}, dimensions={0} | all-to-all | bytes 2097152 | tf_op jit(solution)/shard_map/all_to_all | solution.py:36
  185.2 0.8 all_to_all.25
  185.9 7.4 %all-to-all-start.3 = ((bf16[64,4,512]{2,1,0:T(4,128)(2,1)}), bf16[64,4,512]{2,1,0:T(4,128)(2,1)S(1)}, u32[]{:S(2)}, u32[]{:S(2)}) async-start(bf16[64,4,512]{2,1,0:T(4,128)(2,1)} %all_to_all.25), calls=%async_computation.3 | async-start | bytes 524288 | tf_op jit(solution)/shard_map/all_to_all | solution.py:186
  193.5 1.0 copy.57
  194.4 0.7 mul.171
  195.2 11.2 %all-to-all-done.3 = bf16[64,4,512]{2,1,0:T(4,128)(2,1)S(1)} async-done(((bf16[64,4,512]{2,1,0:T(4,128)(2,1)}), bf16[64,4,512]{2,1,0:T(4,128)(2,1)S(1)}, u32[]{:S(2)}, u32[]{:S(2)}) %all-to-all-start.3) | async-done | bytes 262176 | tf_op jit(solution)/shard_map/all_to_all | solution.py:186
  206.6 0.8 fusion.13
  (50 shorter events, 4.0 us)
Async XLA Ops:
  7.2 156.2 %copy-start = (bf16[1,384,2048]{2,1,0:T(8,128)(2,1)S(1)}, bf16[1,384,2048]{2,1,0:T(8,128)(2,1)}, u32[]{:S(2)}) copy-start(bf16[1,384,2048]{2,1,0:T(8,128)(2,1)} %param.39) | copy-start | bytes 4718596
  7.2 91.0 %copy-start.3 = (bf16[32,2048]{1,0:T(8,128)(2,1)S(1)}, bf16[32,2048]{1,0:T(8,128)(2,1)}, u32[]{:S(2)}) copy-start(bf16[32,2048]{1,0:T(8,128)(2,1)} %param.20) | copy-start | bytes 393220
  7.2 94.1 %copy-start.4 = (f32[32,2,128]{2,1,0:T(2,128)S(1)}, f32[32,2,128]{2,1,0:T(2,128)}, u32[]{:S(2)}) copy-start(f32[32,2,128]{2,1,0:T(2,128)} %param.33) | copy-start | bytes 98308
  7.2 87.6 %all-gather.2.cloned.1.call-start = ((), (), s32[]{:S(2)}) async-start(), calls=%async_computation.4 | async-start | bytes 4259840 | tf_op jit(solution)/shard_map/all_gather | solution.py:15
  14.2 91.5 %copy-start.6 = (f32[32,2]{0,1:T(2,128)}, f32[32,2]{0,1:T(2,128)S(1)}, u32[]{:S(2)}) copy-start(f32[32,2]{0,1:T(2,128)S(1)} %get-tuple-element.10) | copy-start | bytes 772
  105.8 2.0 copy-start.1
  107.8 1.2 copy-start.2
  110.2 13.0 %all-to-all-start = ((bf16[4,32,2048]{2,1,0:T(8,128)(2,1)}), bf16[4,32,2048]{2,1,0:T(8,128)(2,1)S(1)}, u32[]{:S(2)}, u32[]{:S(2)}) async-start(bf16[4,32,2048]{2,1,0:T(8,128)(2,1)} %broadcast_in_dim.8), calls=%async_computation | async-start | bytes 1048576 | tf_op jit(solution)/shard_map/all_to_all | solution.py:20
  167.1 26.2 %copy-start.5 = (f32[32,2]{0,1:T(2,128)S(1)}, f32[32,2]{0,1:T(2,128)}, u32[]{:S(2)}) copy-start(f32[32,2]{0,1:T(2,128)} %param.36) | copy-start | bytes 772
  185.9 20.5 %all-to-all-start.3 = ((bf16[64,4,512]{2,1,0:T(4,128)(2,1)}), bf16[64,4,512]{2,1,0:T(4,128)(2,1)S(1)}, u32[]{:S(2)}, u32[]{:S(2)}) async-start(bf16[64,4,512]{2,1,0:T(4,128)(2,1)} %all_to_all.25), calls=%async_computation.3 | async-start | bytes 524288 | tf_op jit(solution)/shard_map/all_to_all | solution.py:186
Sparse Core Ops, SparseCore 0:
  11.4 83.3 all-gather.1
where the time goes:
time: 215 us; the launch traced here: 214 us
  waiting for transfers between devices  99.2 us (46%)
  blocking collectives  51.6 us (24%)
  matrix products  16.5 us (8%)
  between operations  14.3 us (7%)
  starting transfers between devices  11.4 us (5%)
  local copies, waits for them, and re-layouts  10.7 us (5%)
  other arithmetic  10.5 us (5%)
    all_gather x1, waiting for transfers between devices, in_one_piece(): lax.all_gather(both, axis, axis=dim, tiled=True)  79.1 us
    all_to_all x1, blocking collectives, body(): lax.all_to_all(outgoing, 'ep', split_axis=0, concat_axis=0, tiled=True)  35.2 us
    all_to_all x1, blocking collectives, sum_at_owner(): tiles = lax.all_to_all(split_up(shard, dim, length), axis, 0, 0, tiled=True)  16.5 us
    all_to_all x1, waiting for transfers between devices, body(): lax.all_to_all(half_share, 'ep', split_axis=0, concat_axis=0, tiled=True)  11.2 us
    all_to_all x1, waiting for transfers between devices, copy_for_each(): return lax.all_to_all(copies, axis, split_axis=0, concat_axis=0, tiled=True)  8.98 us
    all_to_all x1, starting transfers between devices, body(): lax.all_to_all(half_share, 'ep', split_axis=0, concat_axis=0, tiled=True)  7.38 us
    dot_general x4, matrix products, body(): jnp.dot(normed, weight_piece, preferred_element_type=jnp.float32)  6.35 us
  transfers between devices with their start and end apart: 3, of which 3 were waited for; matrix products, arithmetic and copies ran while one was open for 4% of the time, Pallas kernels for 0%

commit v1 on v0

v1 whole, which is shorter than its diff:
```python
import functools
import jax
import jax.numpy as jnp
from jax import lax
from jax.experimental import pallas as pl
from jax.experimental.pallas import tpu as pltpu
from jax.sharding import PartitionSpec as P

norm_epsilon = 1e-06
CAP = 4
LANES = 128
F32, BF16 = jnp.float32, jnp.bfloat16
MESH = pl.DeviceIdType.MESH


def iota(shape, dim):
    return lax.broadcasted_iota(jnp.int32, shape, dim)


def dot(a, b):
    return jnp.dot(a, b, preferred_element_type=F32)


def layer_kernel(
    cfg,
    tokens_h, gain_mix_h, gain_ffn_h, wq_h, wk_h, wv_h, wo_h, win_h, wfg_h, bias_in, bias_forget,
    wproj_h, mat_h, nrm_h, stab_h, ids_h, rw_h, wgate_h, wup_h, wdown_h,
    mixed_o, mat_o, nrm_o, stab_o,
    tok, gmix, gffn, win, wfg, wproj, mat, nrm, stab, ids, rw, wgu, wdown,
    wbuf, asend, arecv, psend, precv, normed, square, carry_b, vals_b, num, cell, gain32,
    asrc, adst, resid, table, table_hi, table_lo, dsrc, ddst, xrows0, xrows1, acc, csrc, cdst, own_sum,
    ssrc, sdst, rsrc, rdst,
    sems,
):
    nz, ny, nx, rows, depth, width, ffl, heads = cfg
    ep, t = lax.axis_index("ep"), lax.axis_index("tp")
    c = lax.rem(ep, 2)
    y = lax.rem(lax.div(ep, 2), ny)
    z = lax.div(ep, 2 * ny)
    chips = nz * ny
    quarter = width // nx
    blocks = quarter // LANES
    tile = blocks * CAP
    slots = chips * CAP
    head_dim = LANES
    cols = heads * head_dim

    def at(zz, yy):
        return (lax.rem(zz, nz) * ny + lax.rem(yy, ny)) * 2 + c

    def ahead(d):
        return at(z + lax.div(d, ny), y + lax.rem(d, ny))

    def behind(d):
        return at(z + nz - lax.div(d, ny), y + ny - lax.rem(d, ny))

    partner = ep + 1 - 2 * c
    used = [0]
    sending = []

    def sem():
        used[0] += 1
        return sems.at[used[0] - 1]

    def load(src, dst):
        copy = pltpu.make_async_copy(src, dst, sem())
        copy.start()
        return copy

    def remote(src, dst, to, recv=None):
        copy = pltpu.make_async_remote_copy(
            src_ref=src, dst_ref=dst, send_sem=sem(), recv_sem=sem() if recv is None else recv,
            device_id=to, device_id_type=MESH,
        )
        copy.start()
        sending.append(copy)
        return copy

    weights = [load(w, wbuf.at[z, c, :, i * cols:(i + 1) * cols]) for i, w in enumerate((wq_h, wk_h, wv_h, wo_h))]
    early = [load(a, b) for a, b in ((tokens_h, tok), (gain_mix_h, gmix), (ids_h, ids), (rw_h, rw), (win_h, win), (wfg_h, wfg), (stab_h, stab), (nrm_h, nrm), (gain_ffn_h, gffn))]
    mat_in = load(mat_h, mat)
    wproj_in = load(wproj_h, wproj)
    experts_in = [load(wgate_h.at[0], wgu.at[:, 0:ffl]), load(wup_h.at[0], wgu.at[:, ffl:2 * ffl]), load(wdown_h.at[0], wdown)]

    barrier = pltpu.get_barrier_semaphore()

    def greet(d, carry):
        pl.semaphore_signal(barrier, inc=1, device_id=(ahead(d), t), device_id_type=MESH)
        return carry

    lax.fori_loop(1, chips, greet, 0)
    for dx in range(1, nx):
        pl.semaphore_signal(barrier, inc=1, device_id=(ep, lax.rem(t + dx, nx)), device_id_type=MESH)
    pl.semaphore_signal(barrier, inc=1, device_id=(partner, t), device_id_type=MESH)
    pl.semaphore_wait(barrier, chips - 1 + nx - 1 + 1)

    for copy in weights:
        copy.wait()
    right, left = at(z + 1, y), at(z + nz - 1, y)
    pieces = 2
    pcols = 4 * cols // pieces
    reach = [(nz // 2, nz - 1 - nz // 2), (nz - 1 - nz // 2, nz // 2)]
    handed = sem()

    def piece(zz, p):
        return wbuf.at[lax.rem(zz, nz), c, :, p * pcols:(p + 1) * pcols]

    def hop(zz, p, to, recv):
        return remote(piece(zz, p), piece(zz, p), (to, t), recv)

    going_right, going_left = {}, {}
    recv_right = {(k, p): sem() for p in range(pieces) for k in range(1, reach[p][0] + 1)}
    recv_left = {(k, p): sem() for p in range(pieces) for k in range(1, reach[p][1] + 1)}
    for p in range(pieces):
        if reach[p][0] >= 1:
            going_right[(1, p)] = hop(z, p, right, recv_right[(1, p)])
        if reach[p][1] >= 1:
            going_left[(1, p)] = hop(z, p, left, recv_left[(1, p)])
    for p in range(pieces):
        hop(z, p, partner, handed)

    for copy in early:
        copy.wait()
    wide = tok[...].astype(F32)
    factor = lax.rsqrt(jnp.sum(wide * wide, axis=-1, keepdims=True) * (1.0 / width) + norm_epsilon)
    gain32[0] = gmix[...].astype(F32)
    gain32[1] = gffn[...].astype(F32)
    for b in range(width // LANES):
        here = slice(b * LANES, (b + 1) * LANES)
        normed[:, here] = (tok[:, here].astype(F32) * factor * gain32[0, b:b + 1, :]).astype(BF16)
    share = 2 * depth
    for yy in range(ny):
        if share < LANES:
            per = LANES // share
            for m in range(nz // per):
                parts = []
                for i in range(per):
                    start = ((m * per + i) * ny + yy) * share
                    block = normed[:, start // LANES * LANES:(start // LANES + 1) * LANES].astype(F32)
                    turn = (i * share - start % LANES) % LANES
                    parts.append(pltpu.roll(block, turn, 1) if turn else block)
                lane = iota((rows, LANES), 1)
                merged = parts[0]
                for i in range(1, per):
                    merged = jnp.where(lane >= i * share, parts[i], merged)
                asend[yy, :, m * LANES:(m + 1) * LANES] = merged.astype(BF16)
        else:
            for m in range(nz):
                start = (m * ny + yy) * share
                asend[yy, :, m * share:(m + 1) * share] = normed[:, start:start + share]
    a_copies = []
    for dy in range(1, ny):
        yy = lax.rem(y + dy, ny)
        a_copies.append(remote(asend.at[yy], arecv.at[y], (at(z, yy), t)))
    arecv[y] = asend[y]

    wide_n = blocks * rows
    eid = iota((chips, rows), 0)
    before = (iota((rows, rows), 0) < iota((rows, rows), 1)).astype(F32)
    hot = [(ids[k:k + 1, :] == eid).astype(F32) for k in range(2)]
    totals = jnp.sum(hot[0], axis=1, keepdims=True)
    ranks = [
        jnp.sum(hot[0] * dot(hot[0], before), axis=0, keepdims=True),
        jnp.sum(hot[1] * (dot(hot[1], before) + totals), axis=0, keepdims=True),
    ]
    scale = 1.0 / (rw[0:1, :] + rw[1:2, :])
    row = iota((chips * tile, wide_n), 0)
    lane = iota((chips * tile, wide_n), 1)
    d_of, j_of, s_of = row // tile, row // CAP % blocks, row % CAP
    e_of = (z + d_of // ny) % nz * ny + (y + d_of % ny) % ny
    same = j_of == lane // rows
    hits = []
    for k in range(2):
        ids_t = jnp.concatenate([ids[k:k + 1, :]] * blocks, axis=1)
        rank_t = jnp.concatenate([ranks[k].astype(jnp.int32)] * blocks, axis=1)
        hits.append(same & (e_of == ids_t) & (s_of == rank_t))
    table[...] = (hits[0].astype(F32) + hits[1].astype(F32)).astype(BF16)
    weighted = sum(
        jnp.where(hits[k], jnp.concatenate([rw[k:k + 1, :] * scale] * blocks, axis=1), 0.0) for k in range(2)
    )
    flipped = jnp.transpose(weighted)
    table_hi[...] = flipped.astype(BF16)
    table_lo[...] = (flipped - table_hi[...].astype(F32)).astype(BF16)

    for k in range(1, max(max(reach[0]), max(reach[1])) + 1):
        for p in range(pieces):
            if k <= reach[p][0]:
                going_right[(k, p)].wait_recv()
                if k < reach[p][0]:
                    going_right[(k + 1, p)] = hop(z + nz - k, p, right, recv_right[(k + 1, p)])
                hop(z + nz - k, p, partner, handed)
            if k <= reach[p][1]:
                going_left[(k, p)].wait_recv()
                if k < reach[p][1]:
                    going_left[(k + 1, p)] = hop(z + k, p, left, recv_left[(k + 1, p)])
                hop(z + k, p, partner, handed)

    contract = (((1,), (1,)), ((), ()))
    in_all = lax.dot_general(normed[...], win[...], contract, preferred_element_type=F32)
    forget_all = lax.dot_general(normed[...], wfg[...], contract, preferred_element_type=F32)
    square[...] = jnp.zeros_like(square)
    square[0:heads, 0:rows] = stab[...]
    stab_t = jnp.transpose(square[...])
    gates = []
    for h in range(heads):
        mine = iota(in_all.shape, 1) == t * heads + h
        in_pre = jnp.sum(jnp.where(mine, in_all, 0.0), axis=1, keepdims=True) + bias_in[t * heads + h]
        forget_pre = jnp.sum(jnp.where(mine, forget_all, 0.0), axis=1, keepdims=True) + bias_forget[t * heads + h]
        lf = jnp.minimum(forget_pre, 0.0) - jnp.log1p(jnp.exp(-jnp.abs(forget_pre)))
        old = stab_t[0:rows, h:h + 1]
        new = jnp.maximum(lf + old, in_pre)
        gates.append((new, jnp.exp(lf + old - new), jnp.exp(in_pre - new)))
    for h in range(heads):
        square[0:rows, h:h + 1] = gates[h][0]
    stab_o[...] = jnp.transpose(square[...])[0:heads, 0:rows]

    for copy in a_copies:
        copy.wait_recv()
    whole = wbuf.at[:, 1 - c]
    pltpu.make_async_remote_copy(
        src_ref=whole, dst_ref=whole, send_sem=handed, recv_sem=handed, device_id=(partner, t), device_id_type=MESH
    ).wait_recv()
    features = arecv.shape[2]
    left_side = arecv[...].reshape(ny * rows, features)
    for i in range(4):
        here = slice(i * cols, (i + 1) * cols)
        part = dot(left_side, wbuf[:, :, :, here].reshape(features, cols))
        for yy in range(ny):
            psend[yy, :, here] = part[yy * rows:(yy + 1) * rows].astype(BF16)
    p_copies = []
    for dy in sorted(range(1, ny), key=lambda d: -min(d, ny - d)):
        yy = lax.rem(y + dy, ny)
        p_copies.append(remote(psend.at[yy], precv.at[dy - 1], (at(z, yy), t)))
    total = psend[y].astype(F32)
    for copy in p_copies:
        copy.wait_recv()
    for dy in range(1, ny):
        total = total + precv[dy - 1].astype(F32)
    total = total.astype(BF16).astype(F32)

    mat_in.wait()
    key_scale = head_dim ** -0.5
    query = [total[:, h * head_dim:(h + 1) * head_dim] for h in range(heads)]
    keys = [total[:, cols + h * head_dim:cols + (h + 1) * head_dim] for h in range(heads)]
    for h in range(heads):
        square[h * rows:(h + 1) * rows, :] = query[h]
        square[(heads + h) * rows:(heads + h + 1) * rows, :] = keys[h] * key_scale
    turned = jnp.transpose(square[...])
    for h in range(heads):
        for s in range(rows):
            at_s = h * rows + s
            num[h, s:s + 1, :] = jnp.sum(turned[:, at_s:at_s + 1] * mat[s, h], axis=0, keepdims=True)
    for h in range(heads):
        new, carry, inflow = gates[h]
        kk = keys[h] * key_scale
        vals = total[:, 2 * cols + h * head_dim:2 * cols + (h + 1) * head_dim]
        gate = total[:, 3 * cols + h * head_dim:3 * cols + (h + 1) * head_dim]
        weight = inflow * jnp.sum(query[h] * kk, axis=1, keepdims=True)
        numer = carry * num[h] + weight * vals
        normal = carry * nrm[:, h, :] + inflow * kk
        nrm_o[:, h, :] = normal
        denom = jnp.maximum(jnp.abs(jnp.sum(query[h] * normal, axis=1, keepdims=True)), 1.0)
        hidden = numer / denom * (1.0 / (1.0 + jnp.exp(-gate)))
        cell[:, h * head_dim:(h + 1) * head_dim] = hidden.astype(BF16)
        carry_b[h] = jnp.broadcast_to(carry, (rows, head_dim))
        vals_b[h] = inflow * vals

    wproj_in.wait()
    by_distance = sorted(range(1, nx), key=lambda d: -min(d, nx - d))
    x_copies = []
    for dx in by_distance:
        q = lax.rem(t + dx, nx)
        part = dot(cell[...], wproj[:, pl.ds(pl.multiple_of(q * quarter, quarter), quarter)])
        asrc[dx - 1] = part.astype(BF16)
        x_copies.append(remote(asrc.at[dx - 1], adst.at[dx - 1], (ep, q)))
    mine = pl.ds(pl.multiple_of(t * quarter, quarter), quarter)
    attended = dot(cell[...], wproj[:, mine]).astype(BF16).astype(F32)

    for h in range(heads):
        for s in range(rows):
            at_s = (heads + h) * rows + s
            mat[s, h] = carry_b[h, s:s + 1, :] * mat[s, h] + turned[:, at_s:at_s + 1] * vals_b[h, s:s + 1, :]
    mat_out = load(mat, mat_o)

    for copy in x_copies:
        copy.wait_recv()
    for dx in range(1, nx):
        attended = attended + adst[dx - 1].astype(F32)
    resid_bf = (tok[:, mine].astype(F32) + attended).astype(BF16)
    resid[...] = resid_bf.astype(F32)
    stacked = jnp.concatenate([resid[:, b * LANES:(b + 1) * LANES] for b in range(blocks)], axis=0).astype(BF16)
    packed = dot(table[...], stacked).astype(BF16)
    dsrc[...] = packed
    ddst[0:tile, :] = packed[0:tile]
    d_send, d_recv, r_send, r_recv = sem(), sem(), sem(), sem()

    def tile_of(ref, d):
        return ref.at[pl.ds(pl.multiple_of(d * tile, tile), tile)]

    def send_out(i, carry):
        d = chips - i
        pltpu.make_async_remote_copy(
            src_ref=tile_of(dsrc, d), dst_ref=tile_of(ddst, d), send_sem=d_send, recv_sem=d_recv,
            device_id=(ahead(d), t), device_id_type=MESH,
        ).start()
        return carry

    lax.fori_loop(1, chips, send_out, 0)
    rest = slice(tile, chips * tile)
    d_all = pltpu.make_async_remote_copy(
        src_ref=dsrc.at[rest], dst_ref=ddst.at[rest], send_sem=d_send, recv_sem=d_recv, device_id=(partner, t), device_id_type=MESH
    )

    group = min(16, chips)
    span = group * tile
    per_block = group * CAP
    r_i, c_i = iota((span, span), 0), iota((span, span), 1)
    to_rows = (c_i == r_i % per_block // CAP * tile + r_i // per_block * CAP + r_i % CAP).astype(F32).astype(BF16)
    to_tiles = (c_i == r_i // CAP % blocks * per_block + r_i // tile * CAP + r_i % CAP).astype(F32).astype(BF16)
    for copy in experts_in:
        copy.wait()
    d_all.wait_recv()
    for g in range(chips // group):
        seen = dot(to_rows, ddst[g * span:(g + 1) * span, :]).astype(BF16)
        for b in range(blocks):
            xrows0[0, g * per_block:(g + 1) * per_block, b * LANES:(b + 1) * LANES] = seen[b * per_block:(b + 1) * per_block]

    xg_copies = {dx: remote(xrows0.at[0], xrows0.at[dx], (ep, lax.rem(t + dx, nx))) for dx in by_distance}
    across = {0: remote(xrows0.at[0], xrows1.at[0], (partner, t))}
    squares = [jnp.zeros((slots, 1), F32), jnp.zeros((slots, 1), F32)]

    def take(ref, dx, side):
        q = lax.rem(t + nx - dx, nx)
        fine = []
        for b in range(blocks):
            x = ref[dx, :, b * LANES:(b + 1) * LANES].astype(F32)
            squares[side] = squares[side] + jnp.sum(x * x, axis=1, keepdims=True)
            fine.append((x * gain32[1, pl.ds(q * blocks + b, 1), :]).astype(BF16))
        product = dot(jnp.concatenate(fine, axis=1), wgu[pl.ds(pl.multiple_of(q * quarter, quarter), quarter), :])
        if dx == 0:
            acc[side] = product
        else:
            acc[side] = acc[side] + product

    take(xrows0, 0, 0)
    across[0].wait_recv()
    take(xrows1, 0, 1)
    for dx in reversed(by_distance):
        xg_copies[dx].wait_recv()
        across[dx] = remote(xrows0.at[dx], xrows1.at[dx], (partner, t))
        take(xrows0, dx, 0)
    for dx in reversed(by_distance):
        across[dx].wait_recv()
        take(xrows1, dx, 1)
    inner = []
    for side in range(2):
        factor = lax.rsqrt(squares[side] * (1.0 / width) + norm_epsilon)
        gate, up = acc[side, :, 0:ffl] * factor, acc[side, :, ffl:2 * ffl] * factor
        inner.append((gate * (1.0 / (1.0 + jnp.exp(-gate))) * up).astype(BF16))

    order = by_distance + [0]
    down_copies = {}
    for dx in order:
        q = lax.rem(t + dx, nx)
        wcols = pl.ds(pl.multiple_of(q * quarter, quarter), quarter)
        csrc[dx] = dot(inner[1], wdown[:, wcols]).astype(BF16)
        down_copies[dx] = remote(csrc.at[dx], cdst.at[dx], (partner, t))
    s_copies = []
    for dx in order:
        q = lax.rem(t + dx, nx)
        wcols = pl.ds(pl.multiple_of(q * quarter, quarter), quarter)
        part = dot(inner[0], wdown[:, wcols])
        down_copies[dx].wait_recv()
        part = part + cdst[dx].astype(F32)
        if dx:
            ssrc[dx - 1] = part.astype(BF16)
            s_copies.append(remote(ssrc.at[dx - 1], sdst.at[dx - 1], (ep, q)))
        else:
            own_sum[...] = part
    for copy in s_copies:
        copy.wait_recv()
    back = own_sum[...]
    for dx in range(1, nx):
        back = back + sdst[dx - 1].astype(F32)
    back = back.astype(BF16)

    for g in range(chips // group):
        part = back[g * per_block:(g + 1) * per_block]
        seen = jnp.concatenate([part[:, b * LANES:(b + 1) * LANES] for b in range(blocks)], axis=0)
        rsrc[g * span:(g + 1) * span, :] = dot(to_tiles, seen).astype(BF16)
    rdst[0:tile, :] = rsrc[0:tile, :]

    def send_back(i, carry):
        d = chips - i
        pltpu.make_async_remote_copy(
            src_ref=tile_of(rsrc, d), dst_ref=tile_of(rdst, d), send_sem=r_send, recv_sem=r_recv,
            device_id=(behind(d), t), device_id_type=MESH,
        ).start()
        return carry

    lax.fori_loop(1, chips, send_back, 0)
    r_all = pltpu.make_async_remote_copy(
        src_ref=rsrc.at[rest], dst_ref=rdst.at[rest], send_sem=r_send, recv_sem=r_recv, device_id=(partner, t), device_id_type=MESH
    )
    for copy in sending:
        copy.wait_send()
    d_all.wait_send()
    mat_out.wait()
    r_all.wait_recv()
    routed = dot(table_hi[...], rdst[...]) + dot(table_lo[...], rdst[...])
    for b in range(blocks):
        here = slice(b * LANES, (b + 1) * LANES)
        mixed_o[:, here] = (resid[:, here] + routed[b * rows:(b + 1) * rows]).astype(BF16)
    r_all.wait_send()
    assert used[0] <= sems.shape[0], used


def body(
    tokens, gain_mix, gain_ffn, w_query, w_key, w_value, w_outgate, w_ingate, w_forget, bias_in, bias_forget,
    w_proj, matrix_state, normal_state, stab_state, route_ids, route_weights, w_exp_gate, w_exp_up, w_exp_down,
):
    ep_count, nx = lax.axis_size("ep"), lax.axis_size("tp")
    ny = 4 if ep_count == 64 else 2
    nz = ep_count // 2 // ny
    chips = nz * ny
    rows, width = tokens.shape
    heads, head_dim = matrix_state.shape[1:3]
    depth, cols = w_query.shape
    ffl = w_exp_gate.shape[2]
    quarter = width // nx
    blocks = quarter // LANES
    tile = blocks * CAP
    slots = chips * CAP
    share = 2 * depth * nz
    cfg = (nz, ny, nx, rows, depth, width, ffl, heads)
    hbm = pl.BlockSpec(memory_space=pl.ANY)
    smem = pl.BlockSpec(memory_space=pltpu.SMEM)
    vmem = pl.BlockSpec(memory_space=pltpu.VMEM)
    V = pltpu.VMEM
    xs = max(nx - 1, 1)
    mixed, matrix_new, normal_new, stab_new = pl.pallas_call(
        functools.partial(layer_kernel, cfg),
        out_shape=(
            jax.ShapeDtypeStruct((rows, quarter), BF16),
            jax.ShapeDtypeStruct(matrix_state.shape, F32),
            jax.ShapeDtypeStruct(normal_state.shape, F32),
            jax.ShapeDtypeStruct((heads, rows), F32),
        ),
        in_specs=[hbm] * 9 + [smem] * 2 + [hbm] * 9,
        out_specs=(vmem, hbm, vmem, vmem),
        scratch_shapes=[
            V((rows, width), BF16), V((width // LANES, LANES), BF16), V((width // LANES, LANES), BF16),
            V((nx * heads, width), BF16), V((nx * heads, width), BF16), V((cols, width), BF16),
            V(matrix_state.shape, F32), V(normal_state.shape, F32), V((heads, rows), F32),
            V((2, rows), jnp.int32), V((2, rows), F32), V((width, 2 * ffl), BF16), V((ffl, width), BF16),
            V((nz, 2, depth, 4 * cols), BF16), V((ny, rows, share), BF16), V((ny, rows, share), BF16),
            V((ny, rows, 4 * cols), BF16), V((ny - 1, rows, 4 * cols), BF16), V((rows, width), BF16),
            V((LANES, LANES), F32), V((heads, rows, head_dim), F32), V((heads, rows, head_dim), F32),
            V((heads, rows, head_dim), F32), V((rows, cols), BF16), V((2, width // LANES, LANES), F32),
            V((xs, rows, quarter), BF16), V((xs, rows, quarter), BF16), V((rows, quarter), F32),
            V((chips * tile, blocks * rows), BF16), V((blocks * rows, chips * tile), BF16), V((blocks * rows, chips * tile), BF16),
            V((chips * tile, LANES), BF16), V((chips * tile, LANES), BF16),
            V((nx, slots, quarter), BF16), V((nx, slots, quarter), BF16), V((2, slots, 2 * ffl), F32),
            V((nx, slots, quarter), BF16), V((nx, slots, quarter), BF16), V((slots, quarter), F32),
            V((xs, slots, quarter), BF16), V((xs, slots, quarter), BF16),
            V((chips * tile, LANES), BF16), V((chips * tile, LANES), BF16),
            pltpu.SemaphoreType.DMA((160,)),
        ],
        compiler_params=pltpu.CompilerParams(collective_id=0, has_side_effects=True),
    )(
        tokens, gain_mix.reshape(-1, LANES), gain_ffn.reshape(-1, LANES), w_query, w_key, w_value, w_outgate,
        w_ingate.T, w_forget.T, bias_in, bias_forget, w_proj, matrix_state, normal_state, stab_state.T,
        route_ids.T, route_weights.T, w_exp_gate, w_exp_up, w_exp_down,
    )
    return mixed, matrix_new, normal_new, stab_new.T


def solution(mesh):
    placed = (
        P("ep", None), P(), P(), P("ep", "tp"), P("ep", "tp"), P("ep", "tp"), P("ep", "tp"), P(), P(), P(), P(),
        P("tp", None), P("ep", "tp", None, None), P("ep", "tp", None), P("ep", "tp"), P("ep", None), P("ep", None),
        P("ep", None, "tp"), P("ep", None, "tp"), P("ep", "tp", None),
    )
    return jax.shard_map(
        body,
        mesh=mesh,
        in_specs=placed,
        out_specs=(P("ep", "tp"), P("ep", "tp", None, None), P("ep", "tp", None), P("ep", "tp")),
        check_vma=False,
    )
```

time: 215 us -> 80.4 us (0.37)
  waiting for transfers between devices: 99.2 us -> 0 us
  Pallas kernels: 0 us -> 72.4 us
  blocking collectives: 51.6 us -> 0 us
  matrix products: 16.5 us -> 0 us
  between operations: 14.3 us -> 0.65 us
  starting transfers between devices: 11.4 us -> 0 us
  other arithmetic: 10.5 us -> 0 us
  local copies, waits for them, and re-layouts: 10.7 us -> 7.26 us
    all_gather x1 -> x0, waiting for transfers between devices: 79.1 us -> none  [in_one_piece(): lax.all_gather(both, axis, axis=dim, tiled=True)]
    pallas_call x0 -> x1, Pallas kernels: none -> 72.4 us  [body(): pl.pallas_call(functools.partial(layer_kernel, cfg), out_shape=(jax.Shape...]
    all_to_all x2 -> x0, blocking collectives: 51.6 us -> none  [the longest x1 35.2 us: body(): lax.all_to_all(outgoing, 'ep', split_axis=0, concat_axis=0, tiled=True)]
    all_to_all x2 -> x0, waiting for transfers between devices: 20.1 us -> none  [the longest x1 11.2 us: body(): lax.all_to_all(half_share, 'ep', split_axis=0, concat_axis=0, tiled=True)]
    dot_general x12 -> x0, matrix products: 16.5 us -> none  [the longest x4 6.35 us: body(): jnp.dot(normed, weight_piece, preferred_element_type=jnp.float32)]
    all_to_all x2 -> x0, starting transfers between devices: 11.4 us -> none  [the longest x1 7.38 us: body(): lax.all_to_all(half_share, 'ep', split_axis=0, concat_axis=0, tiled=True)]
    unnamed x15 -> x8, local copies, waits for them, and re-layouts: 3.26 us -> 7.26 us
    add x1 -> x0, other arithmetic: 3.69 us -> none  [memory_step(): carry[..., None, None] * matrix_state]
  transfers between devices with their start and end apart: 3 -> 0, of which waited for: 3 -> 0; matrix products, arithmetic and copies ran while one was open for 4% -> 0% of each run, Pallas kernels for 0% -> 0%
where the time goes in v1:
time: 80.4 us; the launch traced here: 80.3 us
  Pallas kernels  72.4 us (90%)
  local copies, waits for them, and re-layouts  7.26 us (9%)
    pallas_call x1, Pallas kernels, body(): pl.pallas_call(functools.partial(layer_kernel, cfg), out_shape=(jax.Shape...  72.4 us
    unnamed x8, local copies, waits for them, and re-layouts  7.26 us

profile of v1, /device:TPU:1, one launch (start us, length us, event | category | flops | bytes accessed | tf_op | source)
XLA Modules:
  0.0 80.3 jit_solution(15803044818284979680)
XLA Ops:
  0.6 72.4 %shard_map.219 = (bf16[32,512]{1,0:T(8,128)(2,1)}, f32[32,2,128,128]{3,2,1,0:T(8,128)}, f32[32,2,128]{2,1,0:T(2,128)}, f32[2,32]{1,0:T(2,128)}) custom-call(bf16[32,2048]{1,0:T(8,128)(2,1)} %tokens_h.1, bf16[16,128]{1,0:T(8,128)(2,1)} %bitcast.10, bf16[16,128]{1,0:T(8,128)(2,1)} %bitcast.11, bf16[32,256]{1,0:T(8,128)(2,1)} %wq_h.1, bf16[32,256]{1,0:T(8,128)(2,1)} %wk_h.1, ...), custom_call_target="tpu_custom_call" | custom-call | tf_op jit(solution)/shard_map/pallas_call | solution.py:441
  73.0 1.4 %copy.28 = bf16[32,512]{1,0:T(8,128)(2,1)} copy(bf16[32,512]{1,0:T(8,128)(2,1)} %get-tuple-element.16) | data formatting | bytes 65536
  74.4 0.0 copy-start
  74.4 0.0 copy-start.1
  74.4 4.7 %copy.29 = f32[32,2,128,128]{3,2,1,0:T(8,128)} copy(f32[32,2,128,128]{3,2,1,0:T(8,128)} %get-tuple-element.17) | data formatting | bytes 8388608
  79.1 0.0 copy-done
  79.1 0.6 copy.30
  79.7 0.0 copy-done.1
  79.7 0.6 copy.31
Async XLA Ops:
  74.4 4.7 %copy-start = (f32[32,2,128]{2,1,0:T(2,128)S(1)}, f32[32,2,128]{2,1,0:T(2,128)}, u32[]{:S(2)}) copy-start(f32[32,2,128]{2,1,0:T(2,128)} %get-tuple-element.18) | copy-start | bytes 98308
  74.4 5.3 %copy-start.1 = (f32[2,32]{1,0:T(2,128)S(1)}, f32[2,32]{1,0:T(2,128)}, u32[]{:S(2)}) copy-start(f32[2,32]{1,0:T(2,128)} %get-tuple-element.11) | copy-start | bytes 772

commit v2 on v1

--- a/solution.py
+++ b/solution.py
@@ -8,6 +8,8 @@
 
 norm_epsilon = 1e-06
 CAP = 4
+PIECES = 4
+FINISH = 4
 LANES = 128
 F32, BF16 = jnp.float32, jnp.bfloat16
 MESH = pl.DeviceIdType.MESH
@@ -23,10 +25,10 @@
 
 def layer_kernel(
     cfg,
-    tokens_h, gain_mix_h, gain_ffn_h, wq_h, wk_h, wv_h, wo_h, win_h, wfg_h, bias_in, bias_forget,
+    tokens_h, gain_mix_h, gain_ffn_h, wq_h, wk_h, wv_h, wo_h, win_h, wfg_h, bias_in_h, bias_forget_h,
     wproj_h, mat_h, nrm_h, stab_h, ids_h, rw_h, wgate_h, wup_h, wdown_h,
-    mixed_o, mat_o, nrm_o, stab_o,
-    tok, gmix, gffn, win, wfg, wproj, mat, nrm, stab, ids, rw, wgu, wdown,
+    mixed_o, mat, nrm_o, stab_o,
+    tok, gmix, gffn, win, wfg, bias_in, bias_forget, wproj, nrm, stab, ids, rw, wgu, wdown,
     wbuf, asend, arecv, psend, precv, normed, square, carry_b, vals_b, num, cell, gain32,
     asrc, adst, resid, table, table_hi, table_lo, dsrc, ddst, xrows0, xrows1, acc, csrc, cdst, own_sum,
     ssrc, sdst, rsrc, rdst,
@@ -55,6 +57,15 @@
         return at(z + nz - lax.div(d, ny), y + ny - lax.rem(d, ny))
 
     partner = ep + 1 - 2 * c
+    open_scope = []
+
+    def phase(name):
+        if open_scope:
+            open_scope.pop().__exit__(None, None, None)
+        if name:
+            open_scope.append(jax.named_scope(name))
+            open_scope[0].__enter__()
+
     used = [0]
     sending = []
 
@@ -76,12 +87,14 @@
         sending.append(copy)
         return copy
 
+    phase("loads")
     weights = [load(w, wbuf.at[z, c, :, i * cols:(i + 1) * cols]) for i, w in enumerate((wq_h, wk_h, wv_h, wo_h))]
-    early = [load(a, b) for a, b in ((tokens_h, tok), (gain_mix_h, gmix), (ids_h, ids), (rw_h, rw), (win_h, win), (wfg_h, wfg), (stab_h, stab), (nrm_h, nrm), (gain_ffn_h, gffn))]
+    early = [load(a, b) for a, b in ((tokens_h, tok), (gain_mix_h, gmix), (ids_h, ids), (rw_h, rw), (win_h, win), (wfg_h, wfg), (bias_in_h, bias_in), (bias_forget_h, bias_forget), (stab_h, stab), (nrm_h, nrm), (gain_ffn_h, gffn))]
     mat_in = load(mat_h, mat)
     wproj_in = load(wproj_h, wproj)
     experts_in = [load(wgate_h.at[0], wgu.at[:, 0:ffl]), load(wup_h.at[0], wgu.at[:, ffl:2 * ffl]), load(wdown_h.at[0], wdown)]
 
+    phase("barrier")
     barrier = pltpu.get_barrier_semaphore()
 
     def greet(d, carry):
@@ -94,12 +107,14 @@
     pl.semaphore_signal(barrier, inc=1, device_id=(partner, t), device_id_type=MESH)
     pl.semaphore_wait(barrier, chips - 1 + nx - 1 + 1)
 
+    phase("wait_w")
     for copy in weights:
         copy.wait()
+    phase("ring_start")
     right, left = at(z + 1, y), at(z + nz - 1, y)
-    pieces = 2
+    pieces = PIECES
     pcols = 4 * cols // pieces
-    reach = [(nz // 2, nz - 1 - nz // 2), (nz - 1 - nz // 2, nz // 2)]
+    reach = [(nz // 2, nz - 1 - nz // 2), (nz - 1 - nz // 2, nz // 2)] * (pieces // 2)
     handed = sem()
 
     def piece(zz, p):
@@ -119,6 +134,7 @@
     for p in range(pieces):
         hop(z, p, partner, handed)
 
+    phase("norm")
     for copy in early:
         copy.wait()
     wide = tok[...].astype(F32)
@@ -148,12 +164,14 @@
             for m in range(nz):
                 start = (m * ny + yy) * share
                 asend[yy, :, m * share:(m + 1) * share] = normed[:, start:start + share]
+    phase("a_send")
     a_copies = []
     for dy in range(1, ny):
         yy = lax.rem(y + dy, ny)
         a_copies.append(remote(asend.at[yy], arecv.at[y], (at(z, yy), t)))
     arecv[y] = asend[y]
 
+    phase("tables")
     wide_n = blocks * rows
     eid = iota((chips, rows), 0)
     before = (iota((rows, rows), 0) < iota((rows, rows), 1)).astype(F32)
@@ -182,6 +200,7 @@
     table_hi[...] = flipped.astype(BF16)
     table_lo[...] = (flipped - table_hi[...].astype(F32)).astype(BF16)
 
+    phase("ring")
     for k in range(1, max(max(reach[0]), max(reach[1])) + 1):
         for p in range(pieces):
             if k <= reach[p][0]:
@@ -195,6 +214,7 @@
                     going_left[(k + 1, p)] = hop(z + k, p, left, recv_left[(k + 1, p)])
                 hop(z + k, p, partner, handed)
 
+    phase("gates")
     contract = (((1,), (1,)), ((), ()))
     in_all = lax.dot_general(normed[...], win[...], contract, preferred_element_type=F32)
     forget_all = lax.dot_general(normed[...], wfg[...], contract, preferred_element_type=F32)
@@ -204,8 +224,8 @@
     gates = []
     for h in range(heads):
         mine = iota(in_all.shape, 1) == t * heads + h
-        in_pre = jnp.sum(jnp.where(mine, in_all, 0.0), axis=1, keepdims=True) + bias_in[t * heads + h]
-        forget_pre = jnp.sum(jnp.where(mine, forget_all, 0.0), axis=1, keepdims=True) + bias_forget[t * heads + h]
+        in_pre = jnp.sum(jnp.where(mine, in_all + bias_in[...], 0.0), axis=1, keepdims=True)
+        forget_pre = jnp.sum(jnp.where(mine, forget_all + bias_forget[...], 0.0), axis=1, keepdims=True)
         lf = jnp.minimum(forget_pre, 0.0) - jnp.log1p(jnp.exp(-jnp.abs(forget_pre)))
         old = stab_t[0:rows, h:h + 1]
         new = jnp.maximum(lf + old, in_pre)
@@ -214,49 +234,69 @@
         square[0:rows, h:h + 1] = gates[h][0]
     stab_o[...] = jnp.transpose(square[...])[0:heads, 0:rows]
 
+    phase("wait_a")
     for copy in a_copies:
         copy.wait_recv()
+    phase("wait_handed")
     whole = wbuf.at[:, 1 - c]
     pltpu.make_async_remote_copy(
         src_ref=whole, dst_ref=whole, send_sem=handed, recv_sem=handed, device_id=(partner, t), device_id_type=MESH
     ).wait_recv()
+    phase("project")
     features = arecv.shape[2]
     left_side = arecv[...].reshape(ny * rows, features)
+    p_copies = [[], []]
     for i in range(4):
         here = slice(i * cols, (i + 1) * cols)
         part = dot(left_side, wbuf[:, :, :, here].reshape(features, cols))
         for yy in range(ny):
             psend[yy, :, here] = part[yy * rows:(yy + 1) * rows].astype(BF16)
-    p_copies = []
-    for dy in sorted(range(1, ny), key=lambda d: -min(d, ny - d)):
-        yy = lax.rem(y + dy, ny)
-        p_copies.append(remote(psend.at[yy], precv.at[dy - 1], (at(z, yy), t)))
-    total = psend[y].astype(F32)
-    for copy in p_copies:
-        copy.wait_recv()
-    for dy in range(1, ny):
-        total = total + precv[dy - 1].astype(F32)
-    total = total.astype(BF16).astype(F32)
-
+        if i in (0, 3):
+            span = slice(0, cols) if i == 0 else slice(cols, 4 * cols)
+            for dy in sorted(range(1, ny), key=lambda d: -min(d, ny - d)):
+                yy = lax.rem(y + dy, ny)
+                p_copies[i // 3].append(remote(psend.at[yy, :, span], precv.at[dy - 1, :, span], (at(z, yy), t)))
+
+    def summed(half, span):
+        total = psend[y, :, span].astype(F32)
+        for copy in p_copies[half]:
+            copy.wait_recv()
+        for dy in range(1, ny):
+            total = total + precv[dy - 1, :, span].astype(F32)
+        return total.astype(BF16).astype(F32)
+
+    phase("wait_q")
+    q_all = summed(0, slice(0, cols))
+    phase("numer")
     mat_in.wait()
     key_scale = head_dim ** -0.5
-    query = [total[:, h * head_dim:(h + 1) * head_dim] for h in range(heads)]
-    keys = [total[:, cols + h * head_dim:cols + (h + 1) * head_dim] for h in range(heads)]
+    query = [q_all[:, h * head_dim:(h + 1) * head_dim] for h in range(heads)]
+    square[...] = jnp.zeros_like(square)
     for h in range(heads):
         square[h * rows:(h + 1) * rows, :] = query[h]
-        square[(heads + h) * rows:(heads + h + 1) * rows, :] = keys[h] * key_scale
     turned = jnp.transpose(square[...])
     for h in range(heads):
         for s in range(rows):
             at_s = h * rows + s
-            num[h, s:s + 1, :] = jnp.sum(turned[:, at_s:at_s + 1] * mat[s, h], axis=0, keepdims=True)
+            column = turned[:, at_s:at_s + 1]
+            sums = [column[i * 8:(i + 1) * 8] * mat[s, h, i * 8:(i + 1) * 8, :] for i in range(head_dim // 8)]
+            while len(sums) > 1:
+                sums = [sums[i] + sums[i + 1] for i in range(0, len(sums), 2)]
+            num[h, s * 8:(s + 1) * 8, :] = sums[0]
+    phase("wait_kvo")
+    others = summed(1, slice(cols, 4 * cols))
+    keys = [others[:, h * head_dim:(h + 1) * head_dim] for h in range(heads)]
+    phase("cell")
     for h in range(heads):
         new, carry, inflow = gates[h]
         kk = keys[h] * key_scale
-        vals = total[:, 2 * cols + h * head_dim:2 * cols + (h + 1) * head_dim]
-        gate = total[:, 3 * cols + h * head_dim:3 * cols + (h + 1) * head_dim]
+        vals = others[:, cols + h * head_dim:cols + (h + 1) * head_dim]
+        gate = others[:, 2 * cols + h * head_dim:2 * cols + (h + 1) * head_dim]
         weight = inflow * jnp.sum(query[h] * kk, axis=1, keepdims=True)
-        numer = carry * num[h] + weight * vals
+        folded = num[h, pl.ds(0, rows, stride=8), :]
+        for i in range(1, 8):
+            folded = folded + num[h, pl.ds(i, rows, stride=8), :]
+        numer = carry * folded + weight * vals
         normal = carry * nrm[:, h, :] + inflow * kk
         nrm_o[:, h, :] = normal
         denom = jnp.maximum(jnp.abs(jnp.sum(query[h] * normal, axis=1, keepdims=True)), 1.0)
@@ -265,6 +305,7 @@
         carry_b[h] = jnp.broadcast_to(carry, (rows, head_dim))
         vals_b[h] = inflow * vals
 
+    phase("outproj")
     wproj_in.wait()
     by_distance = sorted(range(1, nx), key=lambda d: -min(d, nx - d))
     x_copies = []
@@ -276,14 +317,19 @@
     mine = pl.ds(pl.multiple_of(t * quarter, quarter), quarter)
     attended = dot(cell[...], wproj[:, mine]).astype(BF16).astype(F32)
 
+    phase("update")
+    for h in range(heads):
+        square[h * rows:(h + 1) * rows, :] = keys[h] * key_scale
+    turned = jnp.transpose(square[...])
     for h in range(heads):
         for s in range(rows):
-            at_s = (heads + h) * rows + s
+            at_s = h * rows + s
             mat[s, h] = carry_b[h, s:s + 1, :] * mat[s, h] + turned[:, at_s:at_s + 1] * vals_b[h, s:s + 1, :]
-    mat_out = load(mat, mat_o)
-
+
+    phase("wait_x")
     for copy in x_copies:
         copy.wait_recv()
+    phase("dispatch")
     for dx in range(1, nx):
         attended = attended + adst[dx - 1].astype(F32)
     resid_bf = (tok[:, mine].astype(F32) + attended).astype(BF16)
@@ -295,22 +341,25 @@
     d_send, d_recv, r_send, r_recv = sem(), sem(), sem(), sem()
 
     def tile_of(ref, d):
-        return ref.at[pl.ds(pl.multiple_of(d * tile, tile), tile)]
-
-    def send_out(i, carry):
-        d = chips - i
-        pltpu.make_async_remote_copy(
-            src_ref=tile_of(dsrc, d), dst_ref=tile_of(ddst, d), send_sem=d_send, recv_sem=d_recv,
-            device_id=(ahead(d), t), device_id_type=MESH,
-        ).start()
-        return carry
-
-    lax.fori_loop(1, chips, send_out, 0)
+        return ref.at[d * tile:(d + 1) * tile]
+
+    far = [min(d // ny, nz - d // ny) + min(d % ny, ny - d % ny) for d in range(chips)]
+    far_first = sorted(range(1, chips), key=lambda d: -far[d])
+
+    def scatter(src, dst, send, recv, where):
+        for d in far_first:
+            pltpu.make_async_remote_copy(
+                src_ref=tile_of(src, d), dst_ref=tile_of(dst, d), send_sem=send, recv_sem=recv,
+                device_id=(where(d), t), device_id_type=MESH,
+            ).start()
+
+    scatter(dsrc, ddst, d_send, d_recv, ahead)
     rest = slice(tile, chips * tile)
     d_all = pltpu.make_async_remote_copy(
         src_ref=dsrc.at[rest], dst_ref=ddst.at[rest], send_sem=d_send, recv_sem=d_recv, device_id=(partner, t), device_id_type=MESH
     )
 
+    phase("perms")
     group = min(16, chips)
     span = group * tile
     per_block = group * CAP
@@ -319,14 +368,29 @@
     to_tiles = (c_i == r_i // CAP % blocks * per_block + r_i // tile * CAP + r_i % CAP).astype(F32).astype(BF16)
     for copy in experts_in:
         copy.wait()
+    phase("wait_d")
     d_all.wait_recv()
+    phase("to_rows")
     for g in range(chips // group):
         seen = dot(to_rows, ddst[g * span:(g + 1) * span, :]).astype(BF16)
         for b in range(blocks):
             xrows0[0, g * per_block:(g + 1) * per_block, b * LANES:(b + 1) * LANES] = seen[b * per_block:(b + 1) * per_block]
 
-    xg_copies = {dx: remote(xrows0.at[0], xrows0.at[dx], (ep, lax.rem(t + dx, nx))) for dx in by_distance}
-    across = {0: remote(xrows0.at[0], xrows1.at[0], (partner, t))}
+    phase("gather")
+    parts = 4
+    prow = slots // parts
+    to_right, to_left = (ep, lax.rem(t + 1, nx)), (ep, lax.rem(t + nx - 1, nx))
+    from_x, across = {}, {}
+
+    def prows(ref, dx, p):
+        return ref.at[dx, p * prow:(p + 1) * prow]
+
+    two_way = nx > 2
+    for p in range(parts):
+        from_x[(1, p)] = remote(prows(xrows0, 0, p), prows(xrows0, 1, p), to_right)
+        if two_way:
+            from_x[(nx - 1, p)] = remote(prows(xrows0, 0, p), prows(xrows0, nx - 1, p), to_left)
+    across[0] = remote(xrows0.at[0], xrows1.at[0], (partner, t))
     squares = [jnp.zeros((slots, 1), F32), jnp.zeros((slots, 1), F32)]
 
     def take(ref, dx, side):
@@ -342,46 +406,96 @@
         else:
             acc[side] = acc[side] + product
 
+    def hand(dx):
+        across[dx] = remote(xrows0.at[dx], xrows1.at[dx], (partner, t))
+
     take(xrows0, 0, 0)
+    phase("relay")
+    for p in range(parts):
+        from_x[(1, p)].wait_recv()
+        if two_way and p % 2 == 0:
+            from_x[(2, p)] = remote(prows(xrows0, 1, p), prows(xrows0, 2, p), to_right)
+        if two_way:
+            from_x[(nx - 1, p)].wait_recv()
+            if p % 2 == 1:
+                from_x[(2, p)] = remote(prows(xrows0, nx - 1, p), prows(xrows0, 2, p), to_left)
+    hand(1)
+    if two_way:
+        hand(nx - 1)
     across[0].wait_recv()
+    phase("take_near")
     take(xrows1, 0, 1)
-    for dx in reversed(by_distance):
-        xg_copies[dx].wait_recv()
-        across[dx] = remote(xrows0.at[dx], xrows1.at[dx], (partner, t))
-        take(xrows0, dx, 0)
-    for dx in reversed(by_distance):
-        across[dx].wait_recv()
-        take(xrows1, dx, 1)
+    take(xrows0, 1, 0)
+    if two_way:
+        take(xrows0, nx - 1, 0)
+    across[1].wait_recv()
+    take(xrows1, 1, 1)
+    if two_way:
+        across[nx - 1].wait_recv()
+        take(xrows1, nx - 1, 1)
+        phase("wait_far")
+        for p in range(parts):
+            from_x[(2, p)].wait_recv()
+        hand(2)
+        take(xrows0, 2, 0)
+        phase("wait_far_c")
+        across[2].wait_recv()
+        take(xrows1, 2, 1)
+    phase("inner")
     inner = []
     for side in range(2):
         factor = lax.rsqrt(squares[side] * (1.0 / width) + norm_epsilon)
         gate, up = acc[side, :, 0:ffl] * factor, acc[side, :, ffl:2 * ffl] * factor
         inner.append((gate * (1.0 / (1.0 + jnp.exp(-gate))) * up).astype(BF16))
 
-    order = by_distance + [0]
-    down_copies = {}
+    phase("down1")
+    def down(side, dx):
+        q = lax.rem(t + dx, nx)
+        return dot(inner[side], wdown[:, pl.ds(pl.multiple_of(q * quarter, quarter), quarter)])
+
+    order = ([2, 1, nx - 1] if two_way else [1]) + [0]
+    down_copies, sums = {}, {}
     for dx in order:
-        q = lax.rem(t + dx, nx)
-        wcols = pl.ds(pl.multiple_of(q * quarter, quarter), quarter)
-        csrc[dx] = dot(inner[1], wdown[:, wcols]).astype(BF16)
+        csrc[dx] = down(1, dx).astype(BF16)
         down_copies[dx] = remote(csrc.at[dx], cdst.at[dx], (partner, t))
-    s_copies = []
-    for dx in order:
-        q = lax.rem(t + dx, nx)
-        wcols = pl.ds(pl.multiple_of(q * quarter, quarter), quarter)
-        part = dot(inner[0], wdown[:, wcols])
+    phase("down0")
+    half = slots // 2
+    upper, lower = slice(0, half), slice(half, slots)
+    s_copies = {}
+
+    def both(dx):
+        part = down(0, dx)
         down_copies[dx].wait_recv()
-        part = part + cdst[dx].astype(F32)
-        if dx:
-            ssrc[dx - 1] = part.astype(BF16)
-            s_copies.append(remote(ssrc.at[dx - 1], sdst.at[dx - 1], (ep, q)))
-        else:
-            own_sum[...] = part
-    for copy in s_copies:
-        copy.wait_recv()
-    back = own_sum[...]
-    for dx in range(1, nx):
-        back = back + sdst[dx - 1].astype(F32)
+        return part + cdst[dx].astype(F32)
+
+    if two_way:
+        ssrc[1] = both(2).astype(BF16)
+        s_copies["ur"] = remote(ssrc.at[1, upper], sdst.at[1, upper], to_right)
+        s_copies["ll"] = remote(ssrc.at[1, lower], sdst.at[1, lower], to_left)
+        right_part = both(1)
+        ssrc[0, lower] = right_part[lower].astype(BF16)
+        s_copies["lr"] = remote(ssrc.at[0, lower], sdst.at[0, lower], to_right)
+        left_part = both(nx - 1)
+        ssrc[2, upper] = left_part[upper].astype(BF16)
+        s_copies["ul"] = remote(ssrc.at[2, upper], sdst.at[2, upper], to_left)
+        s_copies["ur"].wait_recv()
+        ssrc[0, upper] = (right_part[upper] + sdst[1, upper].astype(F32)).astype(BF16)
+        s_copies["ur2"] = remote(ssrc.at[0, upper], sdst.at[0, upper], to_right)
+        s_copies["ll"].wait_recv()
+        ssrc[2, lower] = (left_part[lower] + sdst[1, lower].astype(F32)).astype(BF16)
+        s_copies["ll2"] = remote(ssrc.at[2, lower], sdst.at[2, lower], to_left)
+        back = both(0)
+        phase("wait_s")
+        for name in ("lr", "ul", "ur2", "ll2"):
+            s_copies[name].wait_recv()
+        back = back + sdst[0].astype(F32) + sdst[2].astype(F32)
+    else:
+        ssrc[0] = both(1).astype(BF16)
+        s_copies["r"] = remote(ssrc.at[0], sdst.at[0], to_right)
+        back = both(0)
+        s_copies["r"].wait_recv()
+        back = back + sdst[0].astype(F32)
+    phase("to_tiles")
     back = back.astype(BF16)
 
     for g in range(chips // group):
@@ -390,29 +504,39 @@
         rsrc[g * span:(g + 1) * span, :] = dot(to_tiles, seen).astype(BF16)
     rdst[0:tile, :] = rsrc[0:tile, :]
 
-    def send_back(i, carry):
-        d = chips - i
-        pltpu.make_async_remote_copy(
-            src_ref=tile_of(rsrc, d), dst_ref=tile_of(rdst, d), send_sem=r_send, recv_sem=r_recv,
-            device_id=(behind(d), t), device_id_type=MESH,
-        ).start()
-        return carry
-
-    lax.fori_loop(1, chips, send_back, 0)
+    phase("send_back")
+    scatter(rsrc, rdst, r_send, r_recv, behind)
     r_all = pltpu.make_async_remote_copy(
         src_ref=rsrc.at[rest], dst_ref=rdst.at[rest], send_sem=r_send, recv_sem=r_recv, device_id=(partner, t), device_id_type=MESH
     )
+    phase("wait_sends")
     for copy in sending:
         copy.wait_send()
     d_all.wait_send()
-    mat_out.wait()
+    phase("wait_r")
     r_all.wait_recv()
+    phase("combine")
     routed = dot(table_hi[...], rdst[...]) + dot(table_lo[...], rdst[...])
     for b in range(blocks):
         here = slice(b * LANES, (b + 1) * LANES)
         mixed_o[:, here] = (resid[:, here] + routed[b * rows:(b + 1) * rows]).astype(BF16)
     r_all.wait_send()
+    phase(None)
     assert used[0] <= sems.shape[0], used
+
+
+def finish_kernel(mixed, mat, nrm, stab, mixed_o, mat_o, nrm_o, stab_o, sems):
+    per = mat.shape[0] // FINISH
+    copies = [
+        pltpu.make_async_copy(mat.at[i * per:(i + 1) * per], mat_o.at[i * per:(i + 1) * per], sems.at[3 + i])
+        for i in range(FINISH)
+    ]
+    for i, (a, b) in enumerate(((mixed, mixed_o), (nrm, nrm_o), (stab, stab_o))):
+        copies.append(pltpu.make_async_copy(a, b, sems.at[i]))
+    for copy in copies:
+        copy.start()
+    for copy in copies:
+        copy.wait()
 
 
 def body(
@@ -433,12 +557,11 @@
     slots = chips * CAP
     share = 2 * depth * nz
     cfg = (nz, ny, nx, rows, depth, width, ffl, heads)
-    hbm = pl.BlockSpec(memory_space=pl.ANY)
-    smem = pl.BlockSpec(memory_space=pltpu.SMEM)
+    hbm = pl.BlockSpec(memory_space=pltpu.HBM)
     vmem = pl.BlockSpec(memory_space=pltpu.VMEM)
     V = pltpu.VMEM
     xs = max(nx - 1, 1)
-    mixed, matrix_new, normal_new, stab_new = pl.pallas_call(
+    made = pl.pallas_call(
         functools.partial(layer_kernel, cfg),
         out_shape=(
             jax.ShapeDtypeStruct((rows, quarter), BF16),
@@ -446,32 +569,40 @@
             jax.ShapeDtypeStruct(normal_state.shape, F32),
             jax.ShapeDtypeStruct((heads, rows), F32),
         ),
-        in_specs=[hbm] * 9 + [smem] * 2 + [hbm] * 9,
-        out_specs=(vmem, hbm, vmem, vmem),
+        in_specs=[hbm] * 20,
+        out_specs=(vmem,) * 4,
         scratch_shapes=[
             V((rows, width), BF16), V((width // LANES, LANES), BF16), V((width // LANES, LANES), BF16),
-            V((nx * heads, width), BF16), V((nx * heads, width), BF16), V((cols, width), BF16),
-            V(matrix_state.shape, F32), V(normal_state.shape, F32), V((heads, rows), F32),
+            V((nx * heads, width), BF16), V((nx * heads, width), BF16), V((1, nx * heads), F32), V((1, nx * heads), F32), V((cols, width), BF16),
+            V(normal_state.shape, F32), V((heads, rows), F32),
             V((2, rows), jnp.int32), V((2, rows), F32), V((width, 2 * ffl), BF16), V((ffl, width), BF16),
             V((nz, 2, depth, 4 * cols), BF16), V((ny, rows, share), BF16), V((ny, rows, share), BF16),
             V((ny, rows, 4 * cols), BF16), V((ny - 1, rows, 4 * cols), BF16), V((rows, width), BF16),
             V((LANES, LANES), F32), V((heads, rows, head_dim), F32), V((heads, rows, head_dim), F32),
-            V((heads, rows, head_dim), F32), V((rows, cols), BF16), V((2, width // LANES, LANES), F32),
+            V((heads, rows * 8, head_dim), F32), V((rows, cols), BF16), V((2, width // LANES, LANES), F32),
             V((xs, rows, quarter), BF16), V((xs, rows, quarter), BF16), V((rows, quarter), F32),
             V((chips * tile, blocks * rows), BF16), V((blocks * rows, chips * tile), BF16), V((blocks * rows, chips * tile), BF16),
             V((chips * tile, LANES), BF16), V((chips * tile, LANES), BF16),
             V((nx, slots, quarter), BF16), V((nx, slots, quarter), BF16), V((2, slots, 2 * ffl), F32),
-            V((nx, slots, quarter), BF16), V((nx, slots, quarter), BF16), V((slots, quarter), F32),
+            V((nx, slots, quarter), BF16), V((nx, slots, quarter), BF16), V((8, LANES), F32),
             V((xs, slots, quarter), BF16), V((xs, slots, quarter), BF16),
             V((chips * tile, LANES), BF16), V((chips * tile, LANES), BF16),
-            pltpu.SemaphoreType.DMA((160,)),
+            pltpu.SemaphoreType.DMA((240,)),
         ],
-        compiler_params=pltpu.CompilerParams(collective_id=0, has_side_effects=True),
-    )(
+        compiler_params=pltpu.CompilerParams(collective_id=0, has_side_effects=True, vmem_limit_bytes=44 * 1024 * 1024),
+    )(*[pltpu.with_memory_space_constraint(a, pltpu.HBM) for a in (
         tokens, gain_mix.reshape(-1, LANES), gain_ffn.reshape(-1, LANES), w_query, w_key, w_value, w_outgate,
-        w_ingate.T, w_forget.T, bias_in, bias_forget, w_proj, matrix_state, normal_state, stab_state.T,
+        w_ingate.T, w_forget.T, bias_in.reshape(1, -1), bias_forget.reshape(1, -1), w_proj, matrix_state, normal_state, stab_state.T,
         route_ids.T, route_weights.T, w_exp_gate, w_exp_up, w_exp_down,
-    )
+    )])
+    mixed, matrix_new, normal_new, stab_new = pl.pallas_call(
+        finish_kernel,
+        out_shape=[jax.ShapeDtypeStruct(a.shape, a.dtype) for a in made],
+        in_specs=[vmem] * 4,
+        out_specs=[hbm] * 4,
+        scratch_shapes=[pltpu.SemaphoreType.DMA((3 + FINISH,))],
+        compiler_params=pltpu.CompilerParams(vmem_limit_bytes=8 * 1024 * 1024),
+    )(*made)
     return mixed, matrix_new, normal_new, stab_new.T
 
 

time: 80.4 us -> 72 us (0.90)
  the two profiles are of different devices: /device:TPU:1 before, /device:TPU:8 now
where the time goes in v2:
time: 72 us; the launch traced here: 71.9 us
  Pallas kernels  71.2 us (99%)
    pallas_call x1, Pallas kernels, body(): pl.pallas_call(functools.partial(layer_kernel, cfg), out_shape=(jax.Shape...  69.2 us
    pallas_call x1, Pallas kernels, body(): pl.pallas_call(finish_kernel, out_shape=[jax.ShapeDtypeStruct(a.shape, a....  2.08 us

profile of v2, /device:TPU:8, one launch (start us, length us, event | category | flops | bytes accessed | tf_op | source)
XLA Modules:
  0.0 71.9 jit_solution(14235324846428411319)
XLA Ops:
  0.6 69.2 %shard_map.219 = (bf16[32,512]{1,0:T(8,128)(2,1)S(1)}, f32[32,2,128,128]{3,2,1,0:T(8,128)S(1)}, f32[32,2,128]{2,1,0:T(2,128)S(1)}, f32[2,32]{1,0:T(2,128)S(1)}) custom-call(bf16[32,2048]{1,0:T(8,128)(2,1)} %tokens_h.1, bf16[16,128]{1,0:T(8,128)(2,1)} %bitcast.12, bf16[16,128]{1,0:T(8,128)(2,1)} %bitcast.13, bf16[32,256]{1,0:T(8,128)(2,1)} %wq_h.1, ...), custom_call_target="tpu_custom_call" | custom-call | tf_op jit(solution)/shard_map/pallas_call | solution.py:564
  69.8 2.1 %shard_map.220 = (bf16[32,512]{1,0:T(8,128)(2,1)}, f32[32,2,128,128]{3,2,1,0:T(8,128)}, f32[32,2,128]{2,1,0:T(2,128)}, f32[2,32]{1,0:T(2,128)}) custom-call(bf16[32,512]{1,0:T(8,128)(2,1)S(1)} %get-tuple-element.12.mixed, f32[32,2,128,128]{3,2,1,0:T(8,128)S(1)} %get-tuple-element.13.mat, f32[32,2,128]{2,1,0:T(2,128)S(1)} %get-tuple-element.14.nrm, ...), custom_call_target="tpu_custom_call" | custom-call | tf_op jit(solution)/shard_map/pallas_call | solution.py:598
